TPU v7x, 32 devices: a whole 2x2x4 slice. The times are simulated.
32 devices in a mesh: fs: 8 (over z, y), tp: 4 (over x, core).
Axes of the slice: x: 2, y: 2, z: 4, core: 2. Of those that a mesh axis runs over, the one named last changes fastest.
Arguments:
- later_gate: bfloat16 [5120, 5632], P('fs', 'tp'), may hold values from -6 to 6
- later_up: bfloat16 [5120, 5632], P('fs', 'tp'), may hold values from -6 to 6
- early_gate: bfloat16 [5120, 5632], P('fs', 'tp'), may hold values from -6 to 6
- early_up: bfloat16 [5120, 5632], P('fs', 'tp'), may hold values from -6 to 6
- early_cotangent: bfloat16 [5120, 2048], P(('fs', 'tp')), may hold values from -6 to 6
- down_weight: bfloat16 [5632, 2048], P('tp', 'fs'), may hold values from -0.078125 to 0.078125
- grad_running: float32 [5632, 2048], P('tp', 'fs'), may hold values from -224 to 224
Outputs:
- mixed: bfloat16 [5120, 2048], P(('fs', 'tp'))
- gate_grad: bfloat16 [5120, 5632], P('fs', 'tp')
- up_grad: bfloat16 [5120, 5632], P('fs', 'tp')
- grad_total: float32 [5632, 2048], P('tp', 'fs')
All inputs are finite; a program needn't handle non-finite values.
Results may differ from a plain program's by a relative error of at most 0.009.
Values may be sent and summed in bfloat16 or wider, within the bound.
A program may use at most 128 MiB of HBM per device.

v0:
```python
import functools

import jax
import jax.numpy as jnp
from jax import lax
from jax.experimental import pallas as pl
from jax.experimental.pallas import tpu as pltpu
from jax.sharding import PartitionSpec as P

PAIR = 2
F32, BF16 = jnp.float32, jnp.bfloat16


def by_collectives(
    later_gate, later_up, early_gate, early_up, early_cotangent, down_weight, grad_running
):
    later_hidden = (
        jax.nn.silu(later_gate.astype(F32)) * later_up.astype(F32)
    ).astype(BF16)
    gate_value = early_gate.astype(F32)
    up_value = early_up.astype(F32)
    sigma = jax.nn.sigmoid(gate_value)
    early_hidden = (gate_value * sigma * up_value).astype(BF16)
    cot_rows = lax.all_gather(early_cotangent, "tp", axis=0, tiled=True)
    whole = lax.all_gather(down_weight, "fs", axis=1, tiled=True)
    mixed = lax.psum_scatter(
        jnp.dot(later_hidden, whole, preferred_element_type=F32).astype(BF16),
        "tp",
        scatter_dimension=0,
        tiled=True,
    )
    hidden_cot = lax.dot_general(
        cot_rows, whole, (((1,), (1,)), ((), ())), preferred_element_type=F32
    )
    gate_grad = (hidden_cot * up_value * sigma * (1.0 + gate_value * (1.0 - sigma))).astype(BF16)
    up_grad = (hidden_cot * gate_value * sigma).astype(BF16)
    summed = lax.psum_scatter(
        lax.dot_general(
            cot_rows, early_hidden, (((0,), (0,)), ((), ())), preferred_element_type=F32
        ),
        "fs",
        scatter_dimension=0,
        tiled=True,
    )
    return (mixed, gate_grad, up_grad, grad_running + summed.T)


def parts_of(K):
    size = -(-(K // 128) // 4) * 128
    return [(a, min(a + size, K)) for a in range(0, K, size)]


def kernel(
    fs, n,
    lg_ref, lu_ref, eg_ref, eu_ref, cot_ref, w_ref, gr_ref,
    mixed_ref, gg_ref, ug_ref, gt_ref,
    lg, lu, eg, eu, run, W, C, Cp, He, Hl, Gs, Gr, own_g, Ms, Mr, hc, mixed,
    loc, wup_s, wdn_s, wy_s, w_r, c_s, c_r, cy_s, cy_r, cp_s, cp_r, h_s, h_r, g_s, g_r, m_s, m_r,
    wb_s, wb_r, wbu_s, wbd_s,
):
    Z = fs // PAIR
    T, K = lg.shape
    B = W.shape[2]
    R = T // n
    early = max(K * 3 // 22 // 64, 1) * 64
    me_f, me = lax.axis_index("fs"), lax.axis_index("tp")
    z, y = me_f // PAIR, me_f % PAIR
    buddy = {"fs": z * PAIR + 1 - y}

    def remote(src, dst, ss, rs, to):
        return pltpu.make_async_remote_copy(
            src_ref=src, dst_ref=dst, send_sem=ss, recv_sem=rs,
            device_id=to, device_id_type=pl.DeviceIdType.MESH,
        )

    def block(f):
        return pl.ds(pl.multiple_of(f * B, B), B)

    def rows(t):
        return pl.ds(pl.multiple_of(t * R, R), R)

    others_z = [lax.rem(z + k, Z) for k in range(1, Z)]
    others_t = [lax.rem(me + k, n) for k in range(1, n)]

    loads = [
        pltpu.make_async_copy(src, dst, loc.at[i])
        for i, (src, dst) in enumerate((
            (w_ref, W.at[me_f]), (cot_ref, C.at[rows(me), :]), (eg_ref, eg), (eu_ref, eu),
            (lg_ref, lg), (lu_ref, lu), (gr_ref, run),
        ))
    ]
    for copy in loads:
        copy.start()

    barrier = pltpu.get_barrier_semaphore()
    for to in [buddy] + [{"fs": k * PAIR + y} for k in others_z] + [{"tp": t} for t in others_t]:
        pl.semaphore_signal(barrier, inc=1, device_id=to, device_id_type=pl.DeviceIdType.MESH)
    pl.semaphore_wait(barrier, 1 + len(others_z) + len(others_t))

    def up(zz):
        f = zz * PAIR + y
        return remote(W.at[f], W.at[f], wup_s.at[zz], w_r.at[f], {"fs": (z + 1) * PAIR + y})

    def down(zz):
        f = zz * PAIR + y
        return remote(W.at[f], W.at[f], wdn_s.at[zz], w_r.at[f], {"fs": (z - 1) * PAIR + y})

    def across(zz, source=y):
        f = zz * PAIR + source
        part = W.at[f, early:, :]
        return remote(part, part, wy_s.at[zz], w_r.at[f], buddy)

    def first_across():
        part = W.at[me_f, :early, :]
        return remote(part, part, wb_s.at[0], wb_r.at[z], buddy)

    def first_up(zz):
        part = W.at[zz * PAIR + 1 - y, :early, :]
        return remote(part, part, wbu_s.at[zz], wb_r.at[zz], {"fs": (z + 1) * PAIR + y})

    def first_down(zz):
        part = W.at[zz * PAIR + 1 - y, :early, :]
        return remote(part, part, wbd_s.at[zz], wb_r.at[zz], {"fs": (z - 1) * PAIR + y})

    def got_w(f):
        remote(W.at[f], W.at[f], wy_s.at[0], w_r.at[f], buddy).wait_recv()

    loads[0].wait()

    @pl.when(z < Z - 1)
    def _():
        up(z).start()

    @pl.when(z > 0)
    def _():
        down(z).start()

    first_across().start()
    loads[1].wait()
    cy = [
        remote(
            C.at[rows(me), block(k * PAIR + 1 - y)], Cp.at[rows(me), pl.ds(k * B, B)],
            cy_s.at[k], cy_r.at[k], buddy,
        )
        for k in range(Z)
    ]
    for copy in cy:
        copy.start()

    def c_copy(t, f, source):
        part = C.at[rows(source), block(f)]
        return remote(part, part, c_s.at[t * fs + f], c_r.at[source * fs + f], {"tp": t})

    def c_send(side):
        for k in range(Z):
            for t in others_t:
                c_copy(t, k * PAIR + side, me).start()

    def c_wait(side):
        for k in range(Z):
            for t in others_t:
                c_copy(t, k * PAIR + side, t).wait_recv()

    c_send(y)
    step = 32 if T % 32 == 0 else R

    def hidden(g_ref, u_ref, out, a, b):
        @pl.loop(0, T // step)
        def _(i):
            at = pl.ds(pl.multiple_of(i * step, step), step)
            g = g_ref[at, a:b].astype(F32)
            out[at, a:b] = (g * jax.nn.sigmoid(g) * u_ref[at, a:b].astype(F32)).astype(BF16)

    loads[2].wait()
    loads[3].wait()
    swaps = []
    for q, (a, b) in enumerate(parts_of(K)):
        hidden(eg, eu, He.at[0], a, b)
        swaps.append(
            remote(He.at[0, :, a:b], He.at[1, :, a:b], h_s.at[q], h_r.at[q], buddy)
        )
        swaps[-1].start()

    for copy in cy:
        copy.wait_recv()
    for t in others_t:
        remote(Cp.at[rows(me), :], Cp.at[rows(me), :], cp_s.at[t], cp_r.at[me], {"tp": t}).start()
    c_send(1 - y)

    loads[4].wait()
    loads[5].wait()
    hidden(lg, lu, Hl, 0, K)

    def m_copy(f, t):
        return remote(
            Ms.at[rows(t), block(f)], Mr.at[me, :, block(f)],
            m_s.at[f * n + t], m_r.at[f * n + me], {"tp": t},
        )

    def mix(f):
        @pl.loop(0, n)
        def _(t):
            part = jnp.dot(Hl[rows(t), :], W[f], preferred_element_type=F32)
            Ms[rows(t), block(f)] = part.astype(BF16)

        for t in others_t:
            m_copy(f, t).start()

    cuts = [(a, min(a + 512, K)) for a in range(0, K, 512)]

    def back(f, first):
        @pl.loop(0, n)
        def _(t):
            c = C[rows(t), block(f)]
            for a, b in cuts:
                term = lax.dot_general(
                    c, W[f, a:b, :], (((1,), (1,)), ((), ())), preferred_element_type=F32
                )
                hc[rows(t), a:b] = term if first else hc[rows(t), a:b] + term

    def in_order(body, first=0, end=2 * Z - 1):
        @pl.loop(first, end)
        def _(c):
            d = (c + 1) // 2
            zz = jnp.where(c % 2 == 1, z - d, z + d)

            @pl.when((zz >= 0) & (zz < Z))
            def _():
                body(c, zz)

    def relay(c, zz):
        @pl.when(c > 0)
        def _():
            got_w(zz * PAIR + y)

        @pl.when((c > 0) & (zz < z) & (z < Z - 1))
        def _():
            up(zz).start()

        @pl.when((c > 0) & (zz > z) & (z > 0))
        def _():
            down(zz).start()

        part = W.at[zz * PAIR + 1 - y, :early, :]
        remote(part, part, wb_s.at[0], wb_r.at[zz], buddy).wait_recv()

        @pl.when((zz <= z) & (z < Z - 1))
        def _():
            first_up(zz).start()

        @pl.when((zz >= z) & (z > 0))
        def _():
            first_down(zz).start()

        across(zz).start()
        mix(zz * PAIR + y)

    over_rows = (((0,), (0,)), ((), ()))

    def g_copy(q, zz, source):
        a, b = parts_of(K)[q]
        return remote(
            Gs.at[zz, a:b, :], Gr.at[source, a:b, :],
            g_s.at[q * Z + zz], g_r.at[q * Z + source], {"fs": zz * PAIR + y},
        )

    def terms(q):
        swaps[q].wait_recv()
        a, b = parts_of(K)[q]

        @pl.loop(a // 128, b // 128)
        def _(i):
            at = pl.ds(pl.multiple_of(i * 128, 128), 128)
            mine, theirs = He[0, :, at], He[1, :, at]
            for k in range(Z):
                zz = lax.rem(z + k, Z)
                term = lax.dot_general(
                    mine, C[:, block(zz * PAIR + y)], over_rows, preferred_element_type=F32
                ) + lax.dot_general(theirs, Cp[:, block(zz)], over_rows, preferred_element_type=F32)
                if k == 0:
                    own_g[at, :] = term
                else:
                    Gs[zz, at, :] = term.astype(BF16)

        for zz in others_z:
            g_copy(q, zz, z).start()

    parts = len(parts_of(K))
    near = min(5, 2 * Z - 1)
    in_order(relay, 0, near)
    c_wait(y)
    for t in others_t:
        remote(Cp.at[rows(t), :], Cp.at[rows(t), :], cp_s.at[t], cp_r.at[t], {"tp": t}).wait_recv()
    for q in range(parts // 2):
        terms(q)
    in_order(relay, near)
    for q in range(parts // 2, parts):
        terms(q)
    c_wait(1 - y)

    back(z * PAIR + y, True)
    in_order(lambda c, zz: pl.when(c > 0)(lambda: back(zz * PAIR + y, False)))

    def partner(c, zz):
        f = zz * PAIR + 1 - y
        across(zz, 1 - y).wait_recv()
        mix(f)
        back(f, False)

    in_order(partner)

    outs = []

    for t in range(n):
        @pl.loop(t * R // step, (t + 1) * R // step)
        def _(i):
            at = pl.ds(pl.multiple_of(i * step, step), step)
            g, u, h = eg[at, :].astype(F32), eu[at, :].astype(F32), hc[at, :]
            s = jax.nn.sigmoid(g)
            lg[at, :] = (h * u * s * (1.0 + g * (1.0 - s))).astype(BF16)
            lu[at, :] = (h * g * s).astype(BF16)

        at = pl.ds(t * R, R)
        outs.append(pltpu.make_async_copy(lg.at[at, :], gg_ref.at[at, :], loc.at[9 + 2 * t]))
        outs.append(pltpu.make_async_copy(lu.at[at, :], ug_ref.at[at, :], loc.at[10 + 2 * t]))
        outs[-2].start()
        outs[-1].start()

    for q in range(parts):
        for zz in others_z:
            g_copy(q, zz, zz).wait_recv()
    loads[6].wait()

    @pl.loop(0, K // 128)
    def _(i):
        at = pl.ds(pl.multiple_of(i * 128, 128), 128)
        total = own_g[at, :]
        for zz in others_z:
            total = total + Gr[zz, at, :].astype(F32)
        own_g[at, :] = run[at, :] + total

    outs.append(pltpu.make_async_copy(own_g, gt_ref, loc.at[7]))
    outs[-1].start()

    @pl.loop(0, fs)
    def _(f):
        for t in others_t:
            remote(
                Ms.at[rows(t), block(f)], Mr.at[t, :, block(f)],
                m_s.at[f * n + t], m_r.at[f * n + t], {"tp": t},
            ).wait_recv()
        total = Ms[rows(me), block(f)].astype(F32)
        for t in others_t:
            total = total + Mr[t, :, block(f)].astype(F32)
        mixed[:, block(f)] = total.astype(BF16)

    outs.append(pltpu.make_async_copy(mixed, mixed_ref, loc.at[8]))
    outs[-1].start()

    def sent(c, zz):
        @pl.when((zz <= z) & (z < Z - 1))
        def _():
            up(zz).wait_send()
            first_up(zz).wait_send()

        @pl.when((zz >= z) & (z > 0))
        def _():
            down(zz).wait_send()
            first_down(zz).wait_send()

        across(zz).wait_send()

    in_order(sent)
    first_across().wait_send()
    for copy in cy:
        copy.wait_send()
    for t in others_t:
        for f in range(fs):
            c_copy(t, f, me).wait_send()
        remote(Cp.at[rows(me), :], Cp.at[rows(me), :], cp_s.at[t], cp_r.at[me], {"tp": t}).wait_send()
    for copy in swaps:
        copy.wait_send()
    for q in range(parts):
        for zz in others_z:
            g_copy(q, zz, z).wait_send()

    @pl.loop(0, fs)
    def _(f):
        for t in others_t:
            m_copy(f, t).wait_send()

    for copy in outs:
        copy.wait()


def by_kernel(fs, n, *args):
    later_gate, cot, weight = args[0], args[4], args[5]
    T, K = later_gate.shape
    R, D = cot.shape
    B = weight.shape[1]
    Z = fs // PAIR
    parts = len(parts_of(K))
    sem = pltpu.SemaphoreType.DMA
    anywhere = pl.BlockSpec(memory_space=pl.ANY)
    return pl.pallas_call(
        functools.partial(kernel, fs, n),
        out_shape=(
            jax.ShapeDtypeStruct((R, D), BF16),
            jax.ShapeDtypeStruct((T, K), BF16),
            jax.ShapeDtypeStruct((T, K), BF16),
            jax.ShapeDtypeStruct((K, B), F32),
        ),
        in_specs=[anywhere] * 7,
        out_specs=(anywhere,) * 4,
        scratch_shapes=[
            pltpu.VMEM((T, K), BF16), pltpu.VMEM((T, K), BF16),
            pltpu.VMEM((T, K), BF16), pltpu.VMEM((T, K), BF16),
            pltpu.VMEM((K, B), F32),
            pltpu.VMEM((fs, K, B), BF16),
            pltpu.VMEM((T, D), BF16),
            pltpu.VMEM((T, Z * B), BF16),
            pltpu.VMEM((2, T, K), BF16),
            pltpu.VMEM((T, K), BF16),
            pltpu.VMEM((Z, K, B), BF16), pltpu.VMEM((Z, K, B), BF16),
            pltpu.VMEM((K, B), F32),
            pltpu.VMEM((T, D), BF16),
            pltpu.VMEM((n, R, D), BF16),
            pltpu.VMEM((T, K), F32),
            pltpu.VMEM((R, D), BF16),
            sem((9 + 2 * n,)),
            sem((Z,)), sem((Z,)), sem((Z,)), sem((fs,)),
            sem((n * fs,)), sem((n * fs,)), sem((Z,)), sem((Z,)), sem((n,)), sem((n,)),
            sem((parts,)), sem((parts,)), sem((parts * Z,)), sem((parts * Z,)),
            sem((fs * n,)), sem((fs * n,)),
            sem((1,)), sem((Z,)), sem((Z,)), sem((Z,)),
        ],
        compiler_params=pltpu.CompilerParams(
            collective_id=0, has_side_effects=True, vmem_limit_bytes=62 * 2**20
        ),
    )(*args)


def solution(mesh):
    fs, n = mesh.shape["fs"], mesh.shape["tp"]

    def on_device(*args):
        T, K = args[0].shape
        B = args[5].shape[1]
        if fs % PAIR == 0 and fs >= 4 and B % 128 == 0 and K % 128 == 0 and (T // n) % 32 == 0:
            return by_kernel(fs, n, *args)
        return by_collectives(*args)

    placed = (
        P("fs", "tp"),
        P("fs", "tp"),
        P("fs", "tp"),
        P("fs", "tp"),
        P(("fs", "tp"), None),
        P("tp", "fs"),
        P("tp", "fs"),
    )
    return jax.shard_map(
        on_device,
        mesh=mesh,
        in_specs=placed,
        out_specs=(P(("fs", "tp"), None), P("fs", "tp"), P("fs", "tp"), P("tp", "fs")),
        check_vma=False,
    )
```

profile of v0, /device:TPU:9, one launch (start us, length us, event | category | flops | bytes accessed | tf_op | source)
XLA Modules:
  0.0 123.4 jit_solution(507412567779341872)
XLA Ops:
  0.6 114.7 %shard_map.102 = (bf16[160,2048]{1,0:T(8,128)(2,1)}, bf16[640,1408]{1,0:T(8,128)(2,1)}, bf16[640,1408]{1,0:T(8,128)(2,1)}, f32[1408,256]{1,0:T(8,128)}) custom-call(bf16[640,1408]{1,0:T(8,128)(2,1)} %lg_ref.1, bf16[640,1408]{1,0:T(8,128)(2,1)} %lu_ref.1, bf16[640,1408]{1,0:T(8,128)(2,1)} %eg_ref.1, bf16[640,1408]{1,0:T(8,128)(2,1)} %eu_ref.1, ...), custom_call_target="tpu_custom_call" | custom-call | tf_op jit(solution)/shard_map/pallas_call | solution.py:405
  115.4 2.0 %copy.15 = bf16[160,2048]{1,0:T(8,128)(2,1)} copy(bf16[160,2048]{1,0:T(8,128)(2,1)} %get-tuple-element.8) | data formatting | bytes 1310720
  117.3 0.0 copy-start
  117.3 3.0 %copy.16 = bf16[640,1408]{1,0:T(8,128)(2,1)} copy(bf16[640,1408]{1,0:T(8,128)(2,1)} %get-tuple-element.9) | data formatting | bytes 3604480
  120.3 0.0 copy-done
  120.3 0.0 copy-start.1
  120.3 1.2 copy.17
  121.5 0.8 copy-done.1
  122.3 1.1 copy.18
Async XLA Ops:
  117.3 3.0 %copy-start = (bf16[640,1408]{1,0:T(8,128)(2,1)S(1)}, bf16[640,1408]{1,0:T(8,128)(2,1)}, u32[]{:S(2)}) copy-start(bf16[640,1408]{1,0:T(8,128)(2,1)} %get-tuple-element.10) | copy-start | bytes 5406724
  120.3 2.0 %copy-start.1 = (f32[1408,256]{1,0:T(8,128)S(1)}, f32[1408,256]{1,0:T(8,128)}, u32[]{:S(2)}) copy-start(f32[1408,256]{1,0:T(8,128)} %get-tuple-element.11) | copy-start | bytes 4325380
where the time goes:
time: 126 us; the launch traced here: 123 us
  Pallas kernels  115 us (91%)
  local copies, waits for them, and re-layouts  8.07 us (6%)
    pallas_call x1, Pallas kernels, by_kernel(): pl.pallas_call(functools.partial(kernel, fs, n), out_shape=(jax.ShapeDtyp...  115 us
    unnamed x8, local copies, waits for them, and re-layouts  8.07 us

commit v1 on v0

--- a/solution.py
+++ b/solution.py
@@ -54,7 +54,7 @@
     fs, n,
     lg_ref, lu_ref, eg_ref, eu_ref, cot_ref, w_ref, gr_ref,
     mixed_ref, gg_ref, ug_ref, gt_ref,
-    lg, lu, eg, eu, run, W, C, Cp, He, Hl, Gs, Gr, own_g, Ms, Mr, hc, mixed,
+    lg, lu, eg, eu, run, W, C, Cp, He, Hl, Gs, Gr, own_g, Ms, Mr, hc,
     loc, wup_s, wdn_s, wy_s, w_r, c_s, c_r, cy_s, cy_r, cp_s, cp_r, h_s, h_r, g_s, g_r, m_s, m_r,
     wb_s, wb_r, wbu_s, wbd_s,
 ):
@@ -309,22 +309,14 @@
 
     in_order(partner)
 
-    outs = []
-
     for t in range(n):
         @pl.loop(t * R // step, (t + 1) * R // step)
         def _(i):
             at = pl.ds(pl.multiple_of(i * step, step), step)
             g, u, h = eg[at, :].astype(F32), eu[at, :].astype(F32), hc[at, :]
             s = jax.nn.sigmoid(g)
-            lg[at, :] = (h * u * s * (1.0 + g * (1.0 - s))).astype(BF16)
-            lu[at, :] = (h * g * s).astype(BF16)
-
-        at = pl.ds(t * R, R)
-        outs.append(pltpu.make_async_copy(lg.at[at, :], gg_ref.at[at, :], loc.at[9 + 2 * t]))
-        outs.append(pltpu.make_async_copy(lu.at[at, :], ug_ref.at[at, :], loc.at[10 + 2 * t]))
-        outs[-2].start()
-        outs[-1].start()
+            gg_ref[at, :] = (h * u * s * (1.0 + g * (1.0 - s))).astype(BF16)
+            ug_ref[at, :] = (h * g * s).astype(BF16)
 
     for q in range(parts):
         for zz in others_z:
@@ -337,10 +329,7 @@
         total = own_g[at, :]
         for zz in others_z:
             total = total + Gr[zz, at, :].astype(F32)
-        own_g[at, :] = run[at, :] + total
-
-    outs.append(pltpu.make_async_copy(own_g, gt_ref, loc.at[7]))
-    outs[-1].start()
+        gt_ref[at, :] = run[at, :] + total
 
     @pl.loop(0, fs)
     def _(f):
@@ -352,10 +341,7 @@
         total = Ms[rows(me), block(f)].astype(F32)
         for t in others_t:
             total = total + Mr[t, :, block(f)].astype(F32)
-        mixed[:, block(f)] = total.astype(BF16)
-
-    outs.append(pltpu.make_async_copy(mixed, mixed_ref, loc.at[8]))
-    outs[-1].start()
+        mixed_ref[:, block(f)] = total.astype(BF16)
 
     def sent(c, zz):
         @pl.when((zz <= z) & (z < Z - 1))
@@ -389,9 +375,6 @@
         for t in others_t:
             m_copy(f, t).wait_send()
 
-    for copy in outs:
-        copy.wait()
-
 
 def by_kernel(fs, n, *args):
     later_gate, cot, weight = args[0], args[4], args[5]
@@ -405,13 +388,13 @@
     return pl.pallas_call(
         functools.partial(kernel, fs, n),
         out_shape=(
-            jax.ShapeDtypeStruct((R, D), BF16),
-            jax.ShapeDtypeStruct((T, K), BF16),
-            jax.ShapeDtypeStruct((T, K), BF16),
-            jax.ShapeDtypeStruct((K, B), F32),
+            pltpu.VMEM((R, D), BF16),
+            pltpu.VMEM((T, K), BF16),
+            pltpu.VMEM((T, K), BF16),
+            pltpu.VMEM((K, B), F32),
         ),
         in_specs=[anywhere] * 7,
-        out_specs=(anywhere,) * 4,
+        out_specs=(pl.BlockSpec(memory_space=pltpu.VMEM),) * 4,
         scratch_shapes=[
             pltpu.VMEM((T, K), BF16), pltpu.VMEM((T, K), BF16),
             pltpu.VMEM((T, K), BF16), pltpu.VMEM((T, K), BF16),
@@ -426,8 +409,7 @@
             pltpu.VMEM((T, D), BF16),
             pltpu.VMEM((n, R, D), BF16),
             pltpu.VMEM((T, K), F32),
-            pltpu.VMEM((R, D), BF16),
-            sem((9 + 2 * n,)),
+            sem((7,)),
             sem((Z,)), sem((Z,)), sem((Z,)), sem((fs,)),
             sem((n * fs,)), sem((n * fs,)), sem((Z,)), sem((Z,)), sem((n,)), sem((n,)),
             sem((parts,)), sem((parts,)), sem((parts * Z,)), sem((parts * Z,)),
@@ -435,7 +417,7 @@
             sem((1,)), sem((Z,)), sem((Z,)), sem((Z,)),
         ],
         compiler_params=pltpu.CompilerParams(
-            collective_id=0, has_side_effects=True, vmem_limit_bytes=62 * 2**20
+            collective_id=0, has_side_effects=True, vmem_limit_bytes=52 * 2**20
         ),
     )(*args)
 

time: 126 us -> 121 us (0.960)
  local copies, waits for them, and re-layouts: 8.07 us -> 4.37 us
    unnamed x8 -> x4, local copies, waits for them, and re-layouts: 8.07 us -> 4.37 us
where the time goes in v1:
time: 121 us; the launch traced here: 119 us
  Pallas kernels  114 us (94%)
  local copies, waits for them, and re-layouts  4.37 us (4%)
    pallas_call x1, Pallas kernels, by_kernel(): pl.pallas_call(functools.partial(kernel, fs, n), out_shape=(pltpu.VMEM((R...  114 us
    unnamed x4, local copies, waits for them, and re-layouts  4.37 us

profile of v1, /device:TPU:9, one launch (start us, length us, event | category | flops | bytes accessed | tf_op | source)
XLA Modules:
  0.0 119.2 jit_solution(11141900150828638869)
XLA Ops:
  0.6 114.2 %shard_map.102 = (bf16[160,2048]{1,0:T(8,128)(2,1)S(1)}, bf16[640,1408]{1,0:T(8,128)(2,1)S(1)}, bf16[640,1408]{1,0:T(8,128)(2,1)S(1)}, f32[1408,256]{1,0:T(8,128)S(1)}) custom-call(bf16[640,1408]{1,0:T(8,128)(2,1)} %lg_ref.1, bf16[640,1408]{1,0:T(8,128)(2,1)} %lu_ref.1, bf16[640,1408]{1,0:T(8,128)(2,1)} %eg_ref.1, bf16[640,1408]{1,0:T(8,128)(2,1)} %eu_ref.1, ...), custom_call_target="tpu_custom_call" | custom-call | tf_op jit(solution)/shard_map/pallas_call | solution.py:388
  114.8 0.8 copy.15
  115.6 1.1 copy.18
  116.7 1.2 %copy.16 = bf16[640,1408]{1,0:T(8,128)(2,1)} copy(bf16[640,1408]{1,0:T(8,128)(2,1)S(1)} %get-tuple-element.5) | data formatting | bytes 3604480
  117.9 1.2 %copy.17 = bf16[640,1408]{1,0:T(8,128)(2,1)} copy(bf16[640,1408]{1,0:T(8,128)(2,1)S(1)} %get-tuple-element.6) | data formatting | bytes 3604480

commit v2 on v1

v2 whole, which is shorter than its diff:
```python
import functools

import jax
import jax.numpy as jnp
from jax import lax
from jax.experimental import pallas as pl
from jax.experimental.pallas import tpu as pltpu
from jax.sharding import PartitionSpec as P

PAIR = 2
F32, BF16 = jnp.float32, jnp.bfloat16


def by_collectives(
    later_gate, later_up, early_gate, early_up, early_cotangent, down_weight, grad_running
):
    later_hidden = (
        jax.nn.silu(later_gate.astype(F32)) * later_up.astype(F32)
    ).astype(BF16)
    gate_value = early_gate.astype(F32)
    up_value = early_up.astype(F32)
    sigma = jax.nn.sigmoid(gate_value)
    early_hidden = (gate_value * sigma * up_value).astype(BF16)
    cot_rows = lax.all_gather(early_cotangent, "tp", axis=0, tiled=True)
    whole = lax.all_gather(down_weight, "fs", axis=1, tiled=True)
    mixed = lax.psum_scatter(
        jnp.dot(later_hidden, whole, preferred_element_type=F32).astype(BF16),
        "tp",
        scatter_dimension=0,
        tiled=True,
    )
    hidden_cot = lax.dot_general(
        cot_rows, whole, (((1,), (1,)), ((), ())), preferred_element_type=F32
    )
    gate_grad = (hidden_cot * up_value * sigma * (1.0 + gate_value * (1.0 - sigma))).astype(BF16)
    up_grad = (hidden_cot * gate_value * sigma).astype(BF16)
    summed = lax.psum_scatter(
        lax.dot_general(
            cot_rows, early_hidden, (((0,), (0,)), ((), ())), preferred_element_type=F32
        ),
        "fs",
        scatter_dimension=0,
        tiled=True,
    )
    return (mixed, gate_grad, up_grad, grad_running + summed.T)


def cuts_of(a, b, size=256):
    return [(k, min(k + size, b)) for k in range(a, b, size)]


def kernel(
    fs, n,
    lg_ref, lu_ref, eg_ref, eu_ref, cot_ref, w_ref, gr_ref,
    mixed_ref, gg_ref, ug_ref, gt_ref,
    lg, lu, eg, eu, W, C, Cp, He, Hl, Gs, Gr, Ms, Mr, hc,
    loc, wu_s, wd_s, w_r, bu_s, bd_s, by_s, b_r, la_s, la_r, lb_s, lb_r,
    c_s, c_r, cy_s, cy_r, cp_s, cp_r, h_s, h_r, g_s, g_r, m_s, m_r,
):
    Z = fs // PAIR
    T, K = lg.shape
    B = W.shape[2]
    R = T // n
    early = max(K // 2 // 64, 1) * 64
    split = max((early + K) // 2 // 256 * 256, early)
    ready = early // 256 * 256
    parts = cuts_of(0, K)
    me_f, me = lax.axis_index("fs"), lax.axis_index("tp")
    z, y = me_f // PAIR, me_f % PAIR
    buddy = {"fs": z * PAIR + 1 - y}
    above, below = {"fs": (z + 1) * PAIR + y}, {"fs": (z - 1) * PAIR + y}
    has_above, has_below = z < Z - 1, z > 0

    def remote(src, dst, ss, rs, to):
        return pltpu.make_async_remote_copy(
            src_ref=src, dst_ref=dst, send_sem=ss, recv_sem=rs,
            device_id=to, device_id_type=pl.DeviceIdType.MESH,
        )

    def block(f):
        return pl.ds(pl.multiple_of(f * B, B), B)

    def rows(t):
        return pl.ds(pl.multiple_of(t * R, R), R)

    others_t = [lax.rem(me + k, n) for k in range(1, n)]

    loads = [
        pltpu.make_async_copy(src, dst, loc.at[i])
        for i, (src, dst) in enumerate((
            (w_ref, W.at[me_f]), (cot_ref, C.at[rows(me), :]), (eg_ref, eg), (eu_ref, eu),
            (lg_ref, lg), (lu_ref, lu), (gr_ref, gt_ref),
        ))
    ]
    for copy in loads:
        copy.start()

    barrier = pltpu.get_barrier_semaphore()

    def greet(to):
        pl.semaphore_signal(barrier, inc=1, device_id=to, device_id_type=pl.DeviceIdType.MESH)

    pl.when(has_above)(lambda: greet(above))
    pl.when(has_below)(lambda: greet(below))
    for to in [buddy] + [{"tp": t} for t in others_t]:
        greet(to)
    pl.semaphore_wait(barrier, n + has_above.astype(jnp.int32) + has_below.astype(jnp.int32))

    def up(zz):
        f = zz * PAIR + y
        return remote(W.at[f], W.at[f], wu_s.at[zz], w_r.at[zz], above)

    def down(zz):
        f = zz * PAIR + y
        return remote(W.at[f], W.at[f], wd_s.at[zz], w_r.at[zz], below)

    def early_part(zz, side):
        return W.at[zz * PAIR + side, :early, :]

    def early_across():
        part = early_part(z, y)
        return remote(part, part, by_s.at[0], b_r.at[z], buddy)

    def early_up(zz):
        part = early_part(zz, 1 - y)
        return remote(part, part, bu_s.at[zz], b_r.at[zz], above)

    def early_down(zz):
        part = early_part(zz, 1 - y)
        return remote(part, part, bd_s.at[zz], b_r.at[zz], below)

    def late_a(zz, side=y):
        part = W.at[zz * PAIR + side, early:split, :]
        return remote(part, part, la_s.at[zz], la_r.at[zz], buddy)

    def late_b(zz, side=y):
        part = W.at[zz * PAIR + side, split:, :]
        return remote(part, part, lb_s.at[zz], lb_r.at[zz], buddy)

    def passed(zz, go_up, go_down):
        @pl.when((zz <= z) & has_above)
        def _():
            go_up(zz)

        @pl.when((zz >= z) & has_below)
        def _():
            go_down(zz)

    def at_distance(d, body):
        if d == 0:
            body(z)
        else:
            pl.when(z >= d)(lambda: body(z - d))
            pl.when(z + d < Z)(lambda: body(z + d))

    loads[0].wait()
    passed(z, lambda zz: up(zz).start(), lambda zz: down(zz).start())
    loads[1].wait()
    cy = [
        remote(
            C.at[rows(me), block(k * PAIR + 1 - y)], Cp.at[rows(me), pl.ds(k * B, B)],
            cy_s.at[k], cy_r.at[k], buddy,
        )
        for k in range(Z)
    ]
    for copy in cy:
        copy.start()
    early_across().start()

    def c_copy(t, f, source):
        part = C.at[rows(source), block(f)]
        return remote(part, part, c_s.at[t * fs + f], c_r.at[source * fs + f], {"tp": t})

    def c_send(side):
        for k in range(Z):
            for t in others_t:
                c_copy(t, k * PAIR + side, me).start()

    def c_wait(side):
        for k in range(Z):
            for t in others_t:
                c_copy(t, k * PAIR + side, t).wait_recv()

    def cp_copy(t, source):
        part = Cp.at[rows(source), :]
        return remote(part, part, cp_s.at[t], cp_r.at[source], {"tp": t})

    c_send(y)

    loads[2].wait()
    loads[3].wait()
    swaps = []
    for q, (a, b) in enumerate(parts):
        @pl.loop(0, T // 128)
        def _(i):
            at = pl.ds(pl.multiple_of(i * 128, 128), 128)
            g = eg[at, a:b].astype(F32)
            h = g * jax.nn.sigmoid(g) * eu[at, a:b].astype(F32)
            He[0, a:b, at] = h.T.astype(BF16)

        swaps.append(remote(He.at[0, a:b, :], He.at[1, a:b, :], h_s.at[q], h_r.at[q], buddy))
        swaps[-1].start()
    late_a(z).start()

    for copy in cy:
        copy.wait_recv()
    for t in others_t:
        cp_copy(t, me).start()
    c_send(1 - y)

    loads[4].wait()
    loads[5].wait()

    @pl.loop(0, T // 32)
    def _(i):
        at = pl.ds(pl.multiple_of(i * 32, 32), 32)
        g = lg[at, :].astype(F32)
        Hl[at, :] = (g * jax.nn.sigmoid(g) * lu[at, :].astype(F32)).astype(BF16)

    def early_relay(zz):
        part = early_part(zz, 1 - y)
        remote(part, part, by_s.at[0], b_r.at[zz], buddy).wait_recv()
        passed(zz, lambda k: early_up(k).start(), lambda k: early_down(k).start())

    def relay(zz):
        f = zz * PAIR + y
        remote(W.at[f], W.at[f], wu_s.at[zz], w_r.at[zz], buddy).wait_recv()
        passed(zz, lambda k: up(k).start(), lambda k: down(k).start())
        late_a(zz).start()

    def m_copy(f, t):
        return remote(
            Ms.at[rows(t), block(f)], Mr.at[me, :, block(f)],
            m_s.at[f * n + t], m_r.at[f * n + me], {"tp": t},
        )

    def mix(f):
        Ms[:, block(f)] = jnp.dot(Hl[...], W[f], preferred_element_type=F32).astype(BF16)
        for t in others_t:
            m_copy(f, t).start()

    def mixed_sum(f):
        for t in others_t:
            remote(
                Ms.at[rows(t), block(f)], Mr.at[t, :, block(f)],
                m_s.at[f * n + t], m_r.at[f * n + t], {"tp": t},
            ).wait_recv()
        total = Ms[rows(me), block(f)].astype(F32)
        for t in others_t:
            total = total + Mr[t, :, block(f)].astype(F32)
        mixed_ref[:, block(f)] = total.astype(BF16)

    def back(f, a, b, first=False):
        for lo, hi in cuts_of(a, b):
            term = lax.dot_general(
                C[:, block(f)], W[f, lo:hi, :], (((1,), (1,)), ((), ())),
                preferred_element_type=F32,
            )
            hc[:, lo:hi] = term if first else hc[:, lo:hi] + term

    def g_slot(zz, step):
        return jnp.where((step < 0) & (zz == z + step), Z, zz)

    def g_copy(q, zz, step):
        a, b = parts[q]
        slot = g_slot(zz, step)
        return remote(
            Gs.at[zz, a:b, :], Gr.at[slot, a:b, :],
            g_s.at[q * Z + zz], g_r.at[q * (Z + 1) + slot], {"fs": (z + step) * PAIR + y},
        )

    def g_wait(q, slot):
        a, b = parts[q]
        part = Gr.at[slot, a:b, :]
        remote(part, part, g_s.at[0], g_r.at[q * (Z + 1) + slot], buddy).wait_recv()

    def term(q, zz):
        a, b = parts[q]
        return jnp.dot(
            He[0, a:b, :], C[:, block(zz * PAIR + y)], preferred_element_type=F32
        ) + jnp.dot(He[1, a:b, :], Cp[:, block(zz)], preferred_element_type=F32)

    def each_target(body):
        @pl.loop(0, 2 * (Z - 1))
        def _(k):
            step = 1 - 2 * (k % 2)
            zz = z + step * (Z - 1 - k // 2)

            @pl.when((zz >= 0) & (zz < Z))
            def _():
                body(zz, step)

    def grad(q):
        swaps[q].wait_recv()
        a, b = parts[q]

        def onward(zz, step):
            more = jnp.where(step > 0, z > 0, z < Z - 1)

            @pl.when(more)
            def _():
                g_wait(q, zz)

            before = jnp.where(more, Gr[zz, a:b, :].astype(F32), 0.0)
            Gs[zz, a:b, :] = (term(q, zz) + before).astype(BF16)
            g_copy(q, zz, step).start()

        each_target(onward)
        if q == 0:
            loads[6].wait()
        gt_ref[a:b, :] = gt_ref[a:b, :] + term(q, z)

    def grad_end(q):
        a, b = parts[q]

        def add(slot):
            g_wait(q, slot)
            gt_ref[a:b, :] = gt_ref[a:b, :] + Gr[slot, a:b, :].astype(F32)

        pl.when(has_below)(lambda: add(z))
        pl.when(has_above)(lambda: add(Z))

    def finish(a, b):
        @pl.loop(0, T // 32)
        def _(i):
            at = pl.ds(pl.multiple_of(i * 32, 32), 32)
            g, u, h = eg[at, a:b].astype(F32), eu[at, a:b].astype(F32), hc[at, a:b]
            s = jax.nn.sigmoid(g)
            gg_ref[at, a:b] = (h * u * s * (1.0 + g * (1.0 - s))).astype(BF16)
            ug_ref[at, a:b] = (h * g * s).astype(BF16)

    def own(zz):
        return zz * PAIR + y

    def other(zz):
        return zz * PAIR + 1 - y

    early_relay(z)
    mix(own(z))
    todo = list(range(len(parts)))

    def grads(count):
        for q in todo[:count]:
            grad(q)
        del todo[:count]

    for d in range(1, Z):
        at_distance(d, relay)
        if d == Z - 1:
            for k in range(Z):
                at_distance(k, lambda zz: late_b(zz).start())
        at_distance(d, lambda zz: mix(own(zz)))
        if d == 1:
            c_wait(y)
            back(own(z), 0, K, True)
            at_distance(d, early_relay)
            at_distance(d, lambda zz: back(own(zz), 0, K))
            for t in others_t:
                cp_copy(t, t).wait_recv()
            grads(1)
        elif d < Z - 1:
            at_distance(d, lambda zz: back(own(zz), 0, K))
            grads(1)
            at_distance(d, early_relay)
            grads(len(todo) - 1 if d == Z - 2 else 1)
        else:
            at_distance(d, lambda zz: back(own(zz), 0, K))
            grads(len(todo))
            c_wait(1 - y)
            for k in range(d):
                at_distance(k, lambda zz: back(other(zz), 0, ready))
            at_distance(d, early_relay)
            at_distance(d, lambda zz: back(other(zz), 0, ready))

    def got_a(zz):
        late_a(zz, 1 - y).wait_recv()
        back(other(zz), ready, split)

    for d in range(Z):
        at_distance(d, got_a)
    finish(0, split)
    for d in range(Z):
        at_distance(d, lambda zz: mixed_sum(own(zz)))

    def got_b(zz):
        late_b(zz, 1 - y).wait_recv()
        mix(other(zz))
        back(other(zz), split, K)

    for d in range(Z):
        at_distance(d, got_b)
    finish(split, K)
    for q in range(len(parts)):
        grad_end(q)
    for d in range(Z):
        at_distance(d, lambda zz: mixed_sum(other(zz)))

    for d in range(Z):
        def sent(zz):
            passed(zz, lambda k: up(k).wait_send(), lambda k: down(k).wait_send())
            passed(zz, lambda k: early_up(k).wait_send(), lambda k: early_down(k).wait_send())
            late_a(zz).wait_send()
            late_b(zz).wait_send()

        at_distance(d, sent)
    early_across().wait_send()
    for copy in cy:
        copy.wait_send()
    for t in others_t:
        @pl.loop(0, fs)
        def _(f):
            c_copy(t, f, me).wait_send()
            m_copy(f, t).wait_send()

        cp_copy(t, me).wait_send()
    for copy in swaps:
        copy.wait_send()
    for q in range(len(parts)):
        each_target(lambda zz, step: g_copy(q, zz, step).wait_send())


def by_kernel(fs, n, *args):
    later_gate, cot, weight = args[0], args[4], args[5]
    T, K = later_gate.shape
    R, D = cot.shape
    B = weight.shape[1]
    Z = fs // PAIR
    parts = len(cuts_of(0, K))
    sem = pltpu.SemaphoreType.DMA
    anywhere = pl.BlockSpec(memory_space=pl.ANY)
    return pl.pallas_call(
        functools.partial(kernel, fs, n),
        out_shape=(
            pltpu.VMEM((R, D), BF16),
            pltpu.VMEM((T, K), BF16),
            pltpu.VMEM((T, K), BF16),
            pltpu.VMEM((K, B), F32),
        ),
        in_specs=[anywhere] * 7,
        out_specs=(pl.BlockSpec(memory_space=pltpu.VMEM),) * 4,
        scratch_shapes=[
            pltpu.VMEM((T, K), BF16), pltpu.VMEM((T, K), BF16),
            pltpu.VMEM((T, K), BF16), pltpu.VMEM((T, K), BF16),
            pltpu.VMEM((fs, K, B), BF16),
            pltpu.VMEM((T, D), BF16),
            pltpu.VMEM((T, Z * B), BF16),
            pltpu.VMEM((2, K, T), BF16),
            pltpu.VMEM((T, K), BF16),
            pltpu.VMEM((Z, K, B), BF16), pltpu.VMEM((Z + 1, K, B), BF16),
            pltpu.VMEM((T, D), BF16),
            pltpu.VMEM((n, R, D), BF16),
            pltpu.VMEM((T, K), F32),
            sem((7,)),
            sem((Z,)), sem((Z,)), sem((Z,)), sem((Z,)), sem((Z,)), sem((1,)), sem((Z,)),
            sem((Z,)), sem((Z,)), sem((Z,)), sem((Z,)),
            sem((n * fs,)), sem((n * fs,)), sem((Z,)), sem((Z,)), sem((n,)), sem((n,)),
            sem((parts,)), sem((parts,)), sem((parts * Z,)), sem((parts * (Z + 1),)),
            sem((fs * n,)), sem((fs * n,)),
        ],
        compiler_params=pltpu.CompilerParams(
            collective_id=0, has_side_effects=True, vmem_limit_bytes=52 * 2**20
        ),
    )(*args)


def solution(mesh):
    fs, n = mesh.shape["fs"], mesh.shape["tp"]

    def on_device(*args):
        T, K = args[0].shape
        B = args[5].shape[1]
        if (
            fs % PAIR == 0 and fs >= 3 * PAIR and n > 1 and B % 128 == 0 and K % 128 == 0
            and T % 128 == 0 and (T // n) % 32 == 0
        ):
            return by_kernel(fs, n, *args)
        return by_collectives(*args)

    placed = (
        P("fs", "tp"),
        P("fs", "tp"),
        P("fs", "tp"),
        P("fs", "tp"),
        P(("fs", "tp"), None),
        P("tp", "fs"),
        P("tp", "fs"),
    )
    return jax.shard_map(
        on_device,
        mesh=mesh,
        in_specs=placed,
        out_specs=(P(("fs", "tp"), None), P("fs", "tp"), P("fs", "tp"), P("tp", "fs")),
        check_vma=False,
    )
```

time: 121 us -> 113 us (0.934); the launches traced: 119 us -> 113 us
  Pallas kernels: 114 us -> 108 us
    pallas_call x1, Pallas kernels: 114 us -> 108 us  [by_kernel(): pl.pallas_call(functools.partial(kernel, fs, n), out_shape=(pltpu.VMEM((R...]
where the time goes in v2:
time: 113 us
  Pallas kernels  108 us (96%)
  local copies, waits for them, and re-layouts  4.37 us (4%)
    pallas_call x1, Pallas kernels, by_kernel(): pl.pallas_call(functools.partial(kernel, fs, n), out_shape=(pltpu.VMEM((R...  108 us
    unnamed x4, local copies, waits for them, and re-layouts  4.37 us

profile of v2, /device:TPU:9, one launch (start us, length us, event | category | flops | bytes accessed | tf_op | source)
XLA Modules:
  0.0 113.2 jit_solution(13378677759569526900)
XLA Ops:
  0.6 108.2 %shard_map.102 = (bf16[160,2048]{1,0:T(8,128)(2,1)S(1)}, bf16[640,1408]{1,0:T(8,128)(2,1)S(1)}, bf16[640,1408]{1,0:T(8,128)(2,1)S(1)}, f32[1408,256]{1,0:T(8,128)S(1)}) custom-call(bf16[640,1408]{1,0:T(8,128)(2,1)} %lg_ref.1, bf16[640,1408]{1,0:T(8,128)(2,1)} %lu_ref.1, bf16[640,1408]{1,0:T(8,128)(2,1)} %eg_ref.1, bf16[640,1408]{1,0:T(8,128)(2,1)} %eu_ref.1, ...), custom_call_target="tpu_custom_call" | custom-call | tf_op jit(solution)/shard_map/pallas_call | solution.py:431
  108.8 0.8 copy.15
  109.6 1.1 copy.18
  110.7 1.2 %copy.16 = bf16[640,1408]{1,0:T(8,128)(2,1)} copy(bf16[640,1408]{1,0:T(8,128)(2,1)S(1)} %get-tuple-element.5) | data formatting | bytes 3604480
  112.0 1.2 %copy.17 = bf16[640,1408]{1,0:T(8,128)(2,1)} copy(bf16[640,1408]{1,0:T(8,128)(2,1)S(1)} %get-tuple-element.6) | data formatting | bytes 3604480

commit v3 on v2

--- a/solution.py
+++ b/solution.py
@@ -54,7 +54,7 @@
     lg_ref, lu_ref, eg_ref, eu_ref, cot_ref, w_ref, gr_ref,
     mixed_ref, gg_ref, ug_ref, gt_ref,
     lg, lu, eg, eu, W, C, Cp, He, Hl, Gs, Gr, Ms, Mr, hc,
-    loc, wu_s, wd_s, w_r, bu_s, bd_s, by_s, b_r, la_s, la_r, lb_s, lb_r,
+    loc, wu_s, wd_s, w_r, bu_s, bd_s, by_s, b_r, l_s, l_r,
     c_s, c_r, cy_s, cy_r, cp_s, cp_r, h_s, h_r, g_s, g_r, m_s, m_r,
 ):
     Z = fs // PAIR
@@ -62,9 +62,9 @@
     B = W.shape[2]
     R = T // n
     early = max(K // 2 // 64, 1) * 64
-    split = max((early + K) // 2 // 256 * 256, early)
     ready = early // 256 * 256
     parts = cuts_of(0, K)
+    last = len(parts)
     me_f, me = lax.axis_index("fs"), lax.axis_index("tp")
     z, y = me_f // PAIR, me_f % PAIR
     buddy = {"fs": z * PAIR + 1 - y}
@@ -76,6 +76,12 @@
             src_ref=src, dst_ref=dst, send_sem=ss, recv_sem=rs,
             device_id=to, device_id_type=pl.DeviceIdType.MESH,
         )
+
+    def all_sent(part, sem):
+        remote(part, part, sem.at[0], sem.at[0], buddy).wait_send()
+
+    def all_here(part, sem):
+        remote(part, part, sem, sem, buddy).wait_recv()
 
     def block(f):
         return pl.ds(pl.multiple_of(f * B, B), B)
@@ -129,13 +135,18 @@
         part = early_part(zz, 1 - y)
         return remote(part, part, bd_s.at[zz], b_r.at[zz], below)
 
-    def late_a(zz, side=y):
-        part = W.at[zz * PAIR + side, early:split, :]
-        return remote(part, part, la_s.at[zz], la_r.at[zz], buddy)
-
-    def late_b(zz, side=y):
-        part = W.at[zz * PAIR + side, split:, :]
-        return remote(part, part, lb_s.at[zz], lb_r.at[zz], buddy)
+    def late(zz, lo, hi, side=y):
+        part = W.at[zz * PAIR + side, early:, lo:hi]
+        return remote(part, part, l_s.at[0], l_r.at[zz * 2 + lo // (B // 2)], buddy)
+
+    def late_start(zz, d):
+        for lo, hi in cut(d):
+            late(zz, lo, hi).start()
+
+    def cut(d):
+        return whole if d < 2 else halves
+
+    whole, halves = [(0, B)], [(0, B // 2), (B // 2, B)]
 
     def passed(zz, go_up, go_down):
         @pl.when((zz <= z) & has_above)
@@ -156,12 +167,13 @@
     loads[0].wait()
     passed(z, lambda zz: up(zz).start(), lambda zz: down(zz).start())
     loads[1].wait()
+    by_need = [jnp.where(2 * z < Z, Z - 1 - k, k) for k in range(Z)]
     cy = [
         remote(
-            C.at[rows(me), block(k * PAIR + 1 - y)], Cp.at[rows(me), pl.ds(k * B, B)],
-            cy_s.at[k], cy_r.at[k], buddy,
+            C.at[rows(me), block(k * PAIR + 1 - y)], Cp.at[rows(me), block(k)],
+            cy_s.at[0], cy_r.at[k], buddy,
         )
-        for k in range(Z)
+        for k in by_need
     ]
     for copy in cy:
         copy.start()
@@ -169,21 +181,22 @@
 
     def c_copy(t, f, source):
         part = C.at[rows(source), block(f)]
-        return remote(part, part, c_s.at[t * fs + f], c_r.at[source * fs + f], {"tp": t})
+        return remote(part, part, c_s.at[0], c_r.at[f % PAIR], {"tp": t})
 
     def c_send(side):
-        for k in range(Z):
+        for k in by_need:
             for t in others_t:
                 c_copy(t, k * PAIR + side, me).start()
 
     def c_wait(side):
-        for k in range(Z):
-            for t in others_t:
-                c_copy(t, k * PAIR + side, t).wait_recv()
-
-    def cp_copy(t, source):
-        part = Cp.at[rows(source), :]
-        return remote(part, part, cp_s.at[t], cp_r.at[source], {"tp": t})
+        all_here(Mr.at[: n - 1, :, : Z * B], c_r.at[side])
+
+    def cp_copy(t, k, source):
+        part = Cp.at[rows(source), block(k)]
+        return remote(part, part, cp_s.at[0], cp_r.at[k], {"tp": t})
+
+    def cp_wait(k):
+        all_here(Mr.at[: n - 1, :, :B], cp_r.at[k])
 
     c_send(y)
 
@@ -198,14 +211,14 @@
             h = g * jax.nn.sigmoid(g) * eu[at, a:b].astype(F32)
             He[0, a:b, at] = h.T.astype(BF16)
 
-        swaps.append(remote(He.at[0, a:b, :], He.at[1, a:b, :], h_s.at[q], h_r.at[q], buddy))
+        swaps.append(remote(He.at[0, a:b, :], He.at[1, a:b, :], h_s.at[0], h_r.at[q], buddy))
         swaps[-1].start()
-    late_a(z).start()
-
-    for copy in cy:
+    late_start(z, 0)
+
+    for k, copy in zip(by_need, cy):
         copy.wait_recv()
-    for t in others_t:
-        cp_copy(t, me).start()
+        for t in others_t:
+            cp_copy(t, k, me).start()
     c_send(1 - y)
 
     loads[4].wait()
@@ -222,33 +235,39 @@
         remote(part, part, by_s.at[0], b_r.at[zz], buddy).wait_recv()
         passed(zz, lambda k: early_up(k).start(), lambda k: early_down(k).start())
 
-    def relay(zz):
-        f = zz * PAIR + y
-        remote(W.at[f], W.at[f], wu_s.at[zz], w_r.at[zz], buddy).wait_recv()
-        passed(zz, lambda k: up(k).start(), lambda k: down(k).start())
-        late_a(zz).start()
-
-    def m_copy(f, t):
+    def relay(d):
+        def body(zz):
+            f = zz * PAIR + y
+            remote(W.at[f], W.at[f], wu_s.at[zz], w_r.at[zz], buddy).wait_recv()
+            passed(zz, lambda k: up(k).start(), lambda k: down(k).start())
+            late_start(zz, d)
+
+        at_distance(d, body)
+
+    def columns(f, lo, hi):
+        return pl.ds(pl.multiple_of(f * B + lo, B // 2), hi - lo)
+
+    def m_copy(f, t, lo, hi, source):
+        at, i = columns(f, lo, hi), f * 2 + lo // (B // 2)
         return remote(
-            Ms.at[rows(t), block(f)], Mr.at[me, :, block(f)],
-            m_s.at[f * n + t], m_r.at[f * n + me], {"tp": t},
+            Ms.at[rows(t), at], Mr.at[source, :, at],
+            m_s.at[0], m_r.at[i], {"tp": t},
         )
 
-    def mix(f):
-        Ms[:, block(f)] = jnp.dot(Hl[...], W[f], preferred_element_type=F32).astype(BF16)
+    def mix(f, lo=0, hi=B):
+        Ms[:, columns(f, lo, hi)] = jnp.dot(
+            Hl[...], W[f, :, lo:hi], preferred_element_type=F32
+        ).astype(BF16)
         for t in others_t:
-            m_copy(f, t).start()
-
-    def mixed_sum(f):
+            m_copy(f, t, lo, hi, me).start()
+
+    def mixed_sum(f, lo=0, hi=B):
+        at = columns(f, lo, hi)
+        all_here(Mr.at[: n - 1, :, lo:hi], m_r.at[f * 2 + lo // (B // 2)])
+        total = Ms[rows(me), at].astype(F32)
         for t in others_t:
-            remote(
-                Ms.at[rows(t), block(f)], Mr.at[t, :, block(f)],
-                m_s.at[f * n + t], m_r.at[f * n + t], {"tp": t},
-            ).wait_recv()
-        total = Ms[rows(me), block(f)].astype(F32)
-        for t in others_t:
-            total = total + Mr[t, :, block(f)].astype(F32)
-        mixed_ref[:, block(f)] = total.astype(BF16)
+            total = total + Mr[t, :, at].astype(F32)
+        mixed_ref[:, at] = total.astype(BF16)
 
     def back(f, a, b, first=False):
         for lo, hi in cuts_of(a, b):
@@ -266,7 +285,7 @@
         slot = g_slot(zz, step)
         return remote(
             Gs.at[zz, a:b, :], Gr.at[slot, a:b, :],
-            g_s.at[q * Z + zz], g_r.at[q * (Z + 1) + slot], {"fs": (z + step) * PAIR + y},
+            g_s.at[0], g_r.at[q * (Z + 1) + slot], {"fs": (z + step) * PAIR + y},
         )
 
     def g_wait(q, slot):
@@ -290,25 +309,57 @@
             def _():
                 body(zz, step)
 
-    def grad(q):
-        swaps[q].wait_recv()
+    def grad_own(q):
         a, b = parts[q]
-
-        def onward(zz, step):
-            more = jnp.where(step > 0, z > 0, z < Z - 1)
-
-            @pl.when(more)
-            def _():
-                g_wait(q, zz)
-
-            before = jnp.where(more, Gr[zz, a:b, :].astype(F32), 0.0)
-            Gs[zz, a:b, :] = (term(q, zz) + before).astype(BF16)
-            g_copy(q, zz, step).start()
-
-        each_target(onward)
         if q == 0:
             loads[6].wait()
         gt_ref[a:b, :] = gt_ref[a:b, :] + term(q, z)
+
+    def grad_leaf(q):
+        a, b = parts[q]
+
+        def onward(zz, step):
+            if q == 0:
+                cp_wait(zz)
+            Gs[zz, a:b, :] = term(q, zz).astype(BF16)
+            g_copy(q, zz, step).start()
+
+        @pl.when((z == 0) | (z == Z - 1))
+        def _():
+            swaps[q].wait_recv()
+            each_target(onward)
+            if q == 1:
+                cp_wait(z)
+                grad_own(0)
+            if q > 0:
+                grad_own(q)
+
+    def grad_mid(slot):
+        def hop(q, lag):
+            a, b = parts[q]
+
+            def onward(zz, step):
+                @pl.when(jnp.where(step > 0, z, Z - 1 - z) == lag + 1)
+                def _():
+                    g_wait(q, zz)
+                    total = term(q, zz) + Gr[zz, a:b, :].astype(F32)
+                    Gs[zz, a:b, :] = total.astype(BF16)
+                    g_copy(q, zz, step).start()
+
+            each_target(onward)
+
+        @pl.when((z > 0) & (z < Z - 1))
+        def _():
+            if slot == 0:
+                for k in range(Z):
+                    cp_wait(k)
+            if slot < last:
+                swaps[slot].wait_recv()
+            for lag in range(Z - 2):
+                if 0 <= slot - 2 * lag < last:
+                    hop(slot - 2 * lag, lag)
+            if slot < last:
+                grad_own(slot)
 
     def grad_end(q):
         a, b = parts[q]
@@ -335,88 +386,82 @@
     def other(zz):
         return zz * PAIR + 1 - y
 
+    def leaf(a, b):
+        for q in range(a, min(b, last)):
+            grad_leaf(q)
+
+    slots = last + 2 * (Z - 3)
+
+    def mid(a, b):
+        for slot in range(a, min(b, slots)):
+            grad_mid(slot)
+
+    def got(zz, lo, hi):
+        late(zz, lo, hi, 1 - y).wait_recv()
+        mix(other(zz), lo, hi)
+        if hi == B:
+            back(other(zz), ready, K)
+
     early_relay(z)
     mix(own(z))
-    todo = list(range(len(parts)))
-
-    def grads(count):
-        for q in todo[:count]:
-            grad(q)
-        del todo[:count]
-
-    for d in range(1, Z):
-        at_distance(d, relay)
-        if d == Z - 1:
-            for k in range(Z):
-                at_distance(k, lambda zz: late_b(zz).start())
+    relay(1)
+    at_distance(1, lambda zz: mix(own(zz)))
+    c_wait(y)
+    back(own(z), 0, K, True)
+    leaf(0, 1)
+    at_distance(1, early_relay)
+    at_distance(1, lambda zz: back(own(zz), 0, K))
+    leaf(1, 3)
+    mid(0, 2)
+    for d in range(2, Z - 1):
+        relay(d)
         at_distance(d, lambda zz: mix(own(zz)))
-        if d == 1:
-            c_wait(y)
-            back(own(z), 0, K, True)
-            at_distance(d, early_relay)
-            at_distance(d, lambda zz: back(own(zz), 0, K))
-            for t in others_t:
-                cp_copy(t, t).wait_recv()
-            grads(1)
-        elif d < Z - 1:
-            at_distance(d, lambda zz: back(own(zz), 0, K))
-            grads(1)
-            at_distance(d, early_relay)
-            grads(len(todo) - 1 if d == Z - 2 else 1)
-        else:
-            at_distance(d, lambda zz: back(own(zz), 0, K))
-            grads(len(todo))
-            c_wait(1 - y)
-            for k in range(d):
-                at_distance(k, lambda zz: back(other(zz), 0, ready))
-            at_distance(d, early_relay)
-            at_distance(d, lambda zz: back(other(zz), 0, ready))
-
-    def got_a(zz):
-        late_a(zz, 1 - y).wait_recv()
-        back(other(zz), ready, split)
-
-    for d in range(Z):
-        at_distance(d, got_a)
-    finish(0, split)
+        at_distance(d, lambda zz: back(own(zz), 0, K))
+        leaf(d + 1, d + 2)
+        at_distance(d, early_relay)
+    leaf(Z, last)
+    c_wait(1 - y)
+    for d in range(Z - 1):
+        at_distance(d, lambda zz: back(other(zz), 0, ready))
+    mid(2, 3)
+    relay(Z - 1)
+    at_distance(Z - 1, lambda zz: mix(own(zz)))
+    at_distance(Z - 1, lambda zz: back(own(zz), 0, K))
+    mid(3, 4)
+    got(z, 0, B)
+    mid(4, 6)
+    pl.when(has_below)(lambda: got(z - 1, 0, B))
+    mid(6, slots - 1)
+    pl.when(has_above)(lambda: got(z + 1, 0, B))
+    mid(slots - 1, slots)
+    at_distance(Z - 1, early_relay)
+    at_distance(Z - 1, lambda zz: back(other(zz), 0, ready))
+    finish(0, ready)
     for d in range(Z):
         at_distance(d, lambda zz: mixed_sum(own(zz)))
-
-    def got_b(zz):
-        late_b(zz, 1 - y).wait_recv()
-        mix(other(zz))
-        back(other(zz), split, K)
-
-    for d in range(Z):
-        at_distance(d, got_b)
-    finish(split, K)
-    for q in range(len(parts)):
-        grad_end(q)
-    for d in range(Z):
-        at_distance(d, lambda zz: mixed_sum(other(zz)))
-
+    early_across().wait_send()
+    all_sent(Cp.at[rows(me), :], cy_s)
+    all_sent(He.at[0], h_s)
+    all_sent(Mr.at[: n - 1], c_s)
+    all_sent(Mr.at[: n - 1, :, : Z * B], cp_s)
     for d in range(Z):
         def sent(zz):
             passed(zz, lambda k: up(k).wait_send(), lambda k: down(k).wait_send())
             passed(zz, lambda k: early_up(k).wait_send(), lambda k: early_down(k).wait_send())
-            late_a(zz).wait_send()
-            late_b(zz).wait_send()
 
         at_distance(d, sent)
-    early_across().wait_send()
-    for copy in cy:
-        copy.wait_send()
-    for t in others_t:
-        @pl.loop(0, fs)
-        def _(f):
-            c_copy(t, f, me).wait_send()
-            m_copy(f, t).wait_send()
-
-        cp_copy(t, me).wait_send()
-    for copy in swaps:
-        copy.wait_send()
-    for q in range(len(parts)):
-        each_target(lambda zz, step: g_copy(q, zz, step).wait_send())
+    for d in range(2, Z):
+        for lo, hi in cut(d):
+            at_distance(d, lambda zz: got(zz, lo, hi))
+    finish(ready, K)
+    for q in range(last):
+        grad_end(q)
+    all_sent(Gs.at[: Z - 1], g_s)
+    all_sent(W.at[:Z, early:, :], l_s)
+    for d in range(Z):
+        for lo, hi in cut(d):
+            at_distance(d, lambda zz: mixed_sum(other(zz), lo, hi))
+    all_sent(Mr.at[: n - 1], m_s)
 
 
 def by_kernel(fs, n, *args):
@@ -452,10 +497,10 @@
             pltpu.VMEM((T, K), F32),
             sem((7,)),
             sem((Z,)), sem((Z,)), sem((Z,)), sem((Z,)), sem((Z,)), sem((1,)), sem((Z,)),
-            sem((Z,)), sem((Z,)), sem((Z,)), sem((Z,)),
-            sem((n * fs,)), sem((n * fs,)), sem((Z,)), sem((Z,)), sem((n,)), sem((n,)),
-            sem((parts,)), sem((parts,)), sem((parts * Z,)), sem((parts * (Z + 1),)),
-            sem((fs * n,)), sem((fs * n,)),
+            sem((1,)), sem((2 * Z,)),
+            sem((1,)), sem((PAIR,)), sem((1,)), sem((Z,)), sem((1,)), sem((Z,)),
+            sem((1,)), sem((parts,)), sem((1,)), sem((parts * (Z + 1),)),
+            sem((1,)), sem((2 * fs,)),
         ],
         compiler_params=pltpu.CompilerParams(
             collective_id=0, has_side_effects=True, vmem_limit_bytes=52 * 2**20
@@ -470,7 +515,7 @@
         T, K = args[0].shape
         B = args[5].shape[1]
         if (
-            fs % PAIR == 0 and fs >= 3 * PAIR and n > 1 and B % 128 == 0 and K % 128 == 0
+            fs % PAIR == 0 and fs >= 3 * PAIR and n > 1 and B % 256 == 0 and K % 128 == 0 and K > 256
             and T % 128 == 0 and (T // n) % 32 == 0
         ):
             return by_kernel(fs, n, *args)

time: 113 us -> 99.9 us (0.88); the launches traced: 113 us -> 98.7 us
  Pallas kernels: 108 us -> 93.7 us
    pallas_call x1, Pallas kernels: 108 us -> 93.7 us  [by_kernel(): pl.pallas_call(functools.partial(kernel, fs, n), out_shape=(pltpu.VMEM((R...]
where the time goes in v3:
time: 99.9 us; the launch traced here: 98.7 us
  Pallas kernels  93.7 us (94%)
  local copies, waits for them, and re-layouts  4.37 us (4%)
    pallas_call x1, Pallas kernels, by_kernel(): pl.pallas_call(functools.partial(kernel, fs, n), out_shape=(pltpu.VMEM((R...  93.7 us
    unnamed x4, local copies, waits for them, and re-layouts  4.37 us

profile of v3, /device:TPU:9, one launch (start us, length us, event | category | flops | bytes accessed | tf_op | source)
XLA Modules:
  0.0 98.7 jit_solution(13116131830009084662)
XLA Ops:
  0.6 93.7 %shard_map.102 = (bf16[160,2048]{1,0:T(8,128)(2,1)S(1)}, bf16[640,1408]{1,0:T(8,128)(2,1)S(1)}, bf16[640,1408]{1,0:T(8,128)(2,1)S(1)}, f32[1408,256]{1,0:T(8,128)S(1)}) custom-call(bf16[640,1408]{1,0:T(8,128)(2,1)} %lg_ref.1, bf16[640,1408]{1,0:T(8,128)(2,1)} %lu_ref.1, bf16[640,1408]{1,0:T(8,128)(2,1)} %eg_ref.1, bf16[640,1408]{1,0:T(8,128)(2,1)} %eu_ref.1, ...), custom_call_target="tpu_custom_call" | custom-call | tf_op jit(solution)/shard_map/pallas_call | solution.py:476
  94.4 0.8 copy.15
  95.2 1.1 %copy.18 = f32[1408,256]{1,0:T(8,128)} copy(f32[1408,256]{1,0:T(8,128)S(1)} %get-tuple-element.7) | data formatting | bytes 2883584
  96.3 1.2 %copy.16 = bf16[640,1408]{1,0:T(8,128)(2,1)} copy(bf16[640,1408]{1,0:T(8,128)(2,1)S(1)} %get-tuple-element.5) | data formatting | bytes 3604480
  97.5 1.2 %copy.17 = bf16[640,1408]{1,0:T(8,128)(2,1)} copy(bf16[640,1408]{1,0:T(8,128)(2,1)S(1)} %get-tuple-element.6) | data formatting | bytes 3604480

commit v4 on v3

--- a/solution.py
+++ b/solution.py
@@ -61,7 +61,7 @@
     T, K = lg.shape
     B = W.shape[2]
     R = T // n
-    early = max(K // 2 // 64, 1) * 64
+    early = max(K * 45 // 88 // 16, 1) * 16
     ready = early // 256 * 256
     parts = cuts_of(0, K)
     last = len(parts)
@@ -464,6 +464,28 @@
     all_sent(Mr.at[: n - 1], m_s)
 
 
+def store(*refs):
+    count = len(refs) // 2
+    copies = [
+        pltpu.make_async_copy(refs[i], refs[count + i], refs[-1].at[i]) for i in range(count)
+    ]
+    for copy in copies:
+        copy.start()
+    for copy in copies:
+        copy.wait()
+
+
+def to_hbm(arrays):
+    return pl.pallas_call(
+        store,
+        out_shape=tuple(jax.ShapeDtypeStruct(a.shape, a.dtype) for a in arrays),
+        in_specs=[pl.BlockSpec(memory_space=pltpu.VMEM)] * len(arrays),
+        out_specs=(pl.BlockSpec(memory_space=pl.ANY),) * len(arrays),
+        scratch_shapes=[pltpu.SemaphoreType.DMA((len(arrays),))],
+        compiler_params=pltpu.CompilerParams(vmem_limit_bytes=2**20),
+    )(*(pltpu.with_memory_space_constraint(a, pltpu.VMEM) for a in arrays))
+
+
 def by_kernel(fs, n, *args):
     later_gate, cot, weight = args[0], args[4], args[5]
     T, K = later_gate.shape
@@ -473,7 +495,7 @@
     parts = len(cuts_of(0, K))
     sem = pltpu.SemaphoreType.DMA
     anywhere = pl.BlockSpec(memory_space=pl.ANY)
-    return pl.pallas_call(
+    return to_hbm(pl.pallas_call(
         functools.partial(kernel, fs, n),
         out_shape=(
             pltpu.VMEM((R, D), BF16),
@@ -505,7 +527,7 @@
         compiler_params=pltpu.CompilerParams(
             collective_id=0, has_side_effects=True, vmem_limit_bytes=52 * 2**20
         ),
-    )(*args)
+    )(*args))
 
 
 def solution(mesh):

time: 99.9 us -> 97.7 us (0.978)
  local copies, waits for them, and re-layouts: 4.37 us -> 0 us
  Pallas kernels: 93.7 us -> 95.7 us
    unnamed x4 -> x0, local copies, waits for them, and re-layouts: 4.37 us -> none
    pallas_call x0 -> x1, Pallas kernels: none -> 2.54 us  [to_hbm(): pl.pallas_call(store, out_shape=tuple((jax.ShapeDtypeStruct(a.shape, a.dt...]
where the time goes in v4:
time: 97.7 us; the launch traced here: 96.5 us
  Pallas kernels  95.7 us (98%)
    pallas_call x1, Pallas kernels, by_kernel(): pl.pallas_call(functools.partial(kernel, fs, n), out_shape=(pltpu.VMEM((R...  93.2 us
    pallas_call x1, Pallas kernels, to_hbm(): pl.pallas_call(store, out_shape=tuple((jax.ShapeDtypeStruct(a.shape, a.dt...  2.54 us

profile of v4, /device:TPU:9, one launch (start us, length us, event | category | flops | bytes accessed | tf_op | source)
XLA Modules:
  0.0 96.5 jit_solution(1542793430391764509)
XLA Ops:
  0.6 93.2 %shard_map.102 = (bf16[160,2048]{1,0:T(8,128)(2,1)S(1)}, bf16[640,1408]{1,0:T(8,128)(2,1)S(1)}, bf16[640,1408]{1,0:T(8,128)(2,1)S(1)}, f32[1408,256]{1,0:T(8,128)S(1)}) custom-call(bf16[640,1408]{1,0:T(8,128)(2,1)} %lg_ref.1, bf16[640,1408]{1,0:T(8,128)(2,1)} %lu_ref.1, bf16[640,1408]{1,0:T(8,128)(2,1)} %eg_ref.1, bf16[640,1408]{1,0:T(8,128)(2,1)} %eu_ref.1, ...), custom_call_target="tpu_custom_call" | custom-call | tf_op jit(solution)/shard_map/pallas_call | solution.py:498
  93.8 2.5 %shard_map.103 = (bf16[160,2048]{1,0:T(8,128)(2,1)}, bf16[640,1408]{1,0:T(8,128)(2,1)}, bf16[640,1408]{1,0:T(8,128)(2,1)}, f32[1408,256]{1,0:T(8,128)}) custom-call(bf16[160,2048]{1,0:T(8,128)(2,1)S(1)} %get-tuple-element.8.refs_0_, bf16[640,1408]{1,0:T(8,128)(2,1)S(1)} %get-tuple-element.9.refs_1_, bf16[640,1408]{1,0:T(8,128)(2,1)S(1)} %get-tuple-element.10.refs_2_, ...), custom_call_target="tpu_custom_call" | custom-call | tf_op jit(solution)/shard_map/pallas_call | solution.py:479

commit v5 on v4

--- a/solution.py
+++ b/solution.py
@@ -53,7 +53,7 @@
     fs, n,
     lg_ref, lu_ref, eg_ref, eu_ref, cot_ref, w_ref, gr_ref,
     mixed_ref, gg_ref, ug_ref, gt_ref,
-    lg, lu, eg, eu, W, C, Cp, He, Hl, Gs, Gr, Ms, Mr, hc,
+    lg, lu, eg, eu, W, C, Cp, He, Hl, Gs, Gr, Ms, Mr, hc, Ma,
     loc, wu_s, wd_s, w_r, bu_s, bd_s, by_s, b_r, l_s, l_r,
     c_s, c_r, cy_s, cy_r, cp_s, cp_r, h_s, h_r, g_s, g_r, m_s, m_r,
 ):
@@ -254,10 +254,14 @@
             m_s.at[0], m_r.at[i], {"tp": t},
         )
 
-    def mix(f, lo=0, hi=B):
-        Ms[:, columns(f, lo, hi)] = jnp.dot(
-            Hl[...], W[f, :, lo:hi], preferred_element_type=F32
-        ).astype(BF16)
+    def mix(f, lo=0, hi=B, begun=None):
+        if begun is None:
+            total = jnp.dot(Hl[...], W[f, :, lo:hi], preferred_element_type=F32)
+        else:
+            total = begun + jnp.dot(
+                Hl[:, ready:], W[f, ready:, lo:hi], preferred_element_type=F32
+            )
+        Ms[:, columns(f, lo, hi)] = total.astype(BF16)
         for t in others_t:
             m_copy(f, t, lo, hi, me).start()
 
@@ -396,9 +400,14 @@
         for slot in range(a, min(b, slots)):
             grad_mid(slot)
 
-    def got(zz, lo, hi):
+    def begin(zz):
+        Ma[zz] = jnp.dot(
+            Hl[:, :ready], W[other(zz), :ready, :], preferred_element_type=F32
+        )
+
+    def got(zz, lo, hi, begun=False):
         late(zz, lo, hi, 1 - y).wait_recv()
-        mix(other(zz), lo, hi)
+        mix(other(zz), lo, hi, Ma[zz, :, lo:hi] if begun else None)
         if hi == B:
             back(other(zz), ready, K)
 
@@ -437,6 +446,8 @@
     at_distance(Z - 1, early_relay)
     at_distance(Z - 1, lambda zz: back(other(zz), 0, ready))
     finish(0, ready)
+    for d in range(2, Z):
+        at_distance(d, begin)
     for d in range(Z):
         at_distance(d, lambda zz: mixed_sum(own(zz)))
     early_across().wait_send()
@@ -452,7 +463,7 @@
         at_distance(d, sent)
     for d in range(2, Z):
         for lo, hi in cut(d):
-            at_distance(d, lambda zz: got(zz, lo, hi))
+            at_distance(d, lambda zz: got(zz, lo, hi, True))
     finish(ready, K)
     for q in range(last):
         grad_end(q)
@@ -517,6 +528,7 @@
             pltpu.VMEM((T, D), BF16),
             pltpu.VMEM((n, R, D), BF16),
             pltpu.VMEM((T, K), F32),
+            pltpu.VMEM((Z, T, B), F32),
             sem((7,)),
             sem((Z,)), sem((Z,)), sem((Z,)), sem((Z,)), sem((Z,)), sem((1,)), sem((Z,)),
             sem((1,)), sem((2 * Z,)),

time: 97.7 us -> 97.4 us (level)
  no operation moved by 1% of the time
where the time goes in v5:
time: 97.4 us; the launch traced here: 96.3 us
  Pallas kernels  95.4 us (98%)
    pallas_call x1, Pallas kernels, by_kernel(): pl.pallas_call(functools.partial(kernel, fs, n), out_shape=(pltpu.VMEM((R...  92.9 us
    pallas_call x1, Pallas kernels, to_hbm(): pl.pallas_call(store, out_shape=tuple((jax.ShapeDtypeStruct(a.shape, a.dt...  2.54 us

profile of v5, /device:TPU:9, one launch (start us, length us, event | category | flops | bytes accessed | tf_op | source)
XLA Modules:
  0.0 96.3 jit_solution(13070115460455428609)
XLA Ops:
  0.6 92.9 %shard_map.102 = (bf16[160,2048]{1,0:T(8,128)(2,1)S(1)}, bf16[640,1408]{1,0:T(8,128)(2,1)S(1)}, bf16[640,1408]{1,0:T(8,128)(2,1)S(1)}, f32[1408,256]{1,0:T(8,128)S(1)}) custom-call(bf16[640,1408]{1,0:T(8,128)(2,1)} %lg_ref.1, bf16[640,1408]{1,0:T(8,128)(2,1)} %lu_ref.1, bf16[640,1408]{1,0:T(8,128)(2,1)} %eg_ref.1, bf16[640,1408]{1,0:T(8,128)(2,1)} %eu_ref.1, ...), custom_call_target="tpu_custom_call" | custom-call | tf_op jit(solution)/shard_map/pallas_call | solution.py:509
  93.5 2.5 %shard_map.103 = (bf16[160,2048]{1,0:T(8,128)(2,1)}, bf16[640,1408]{1,0:T(8,128)(2,1)}, bf16[640,1408]{1,0:T(8,128)(2,1)}, f32[1408,256]{1,0:T(8,128)}) custom-call(bf16[160,2048]{1,0:T(8,128)(2,1)S(1)} %get-tuple-element.8.refs_0_, bf16[640,1408]{1,0:T(8,128)(2,1)S(1)} %get-tuple-element.9.refs_1_, bf16[640,1408]{1,0:T(8,128)(2,1)S(1)} %get-tuple-element.10.refs_2_, ...), custom_call_target="tpu_custom_call" | custom-call | tf_op jit(solution)/shard_map/pallas_call | solution.py:490
